TPU v7x, 32 devices: a whole 2x2x4 slice. The times are simulated.
32 devices in a mesh: kv: 4 (over y, x), tp: 8 (over z, core).
Axes of the slice: x: 2, y: 2, z: 4, core: 2. Of those that a mesh axis runs over, the one named last changes fastest.
Arguments:
- tokens: bfloat16 [128, 4096], P(None, 'tp'), may hold values from -6 to 6
- norm_gain: float32 [4096], P('tp'), may hold values from 0.1 to 1.9
- query_weight: bfloat16 [4096, 2048], P('tp', 'kv'), may hold values from -0.09375 to 0.09375
- key_weight: bfloat16 [4096, 2048], P('tp', 'kv'), may hold values from -0.09375 to 0.09375
- value_weight: bfloat16 [4096, 2048], P('tp', 'kv'), may hold values from -0.09375 to 0.09375
- input_gate_weight: bfloat16 [4096, 16], P('tp'), may hold values from -0.09375 to 0.09375
- forget_gate_weight: bfloat16 [4096, 16], P('tp'), may hold values from -0.09375 to 0.09375
- input_gate_bias: float32 [16], P('kv'), may hold values from -2 to 2
- forget_gate_bias: float32 [16], P('kv'), may hold values from 1 to 6
- memory_state: float32 [128, 16, 128, 128], P('tp', 'kv'), may hold values from -12 to 12
- normalizer_state: float32 [128, 16, 128], P('tp', 'kv'), may hold values from -24 to 24
- stabilizer_state: float32 [128, 16], P('tp', 'kv'), may hold values from -1 to 3
- block_keys: bfloat16 [128, 16, 128, 128], P('tp', 'kv'), may hold values from -6 to 6
- block_values: bfloat16 [128, 16, 128, 128], P('tp', 'kv'), may hold values from -6 to 6
- block_input_pre: float32 [128, 16, 128], P('tp', 'kv'), may hold values from -6 to 6
- block_forget_pre: float32 [128, 16, 128], P('tp', 'kv'), may hold values from -6 to 6
- block_lengths: int32 [128], P('tp'), may hold values from 1 to 128, 6553 in all
- head_norm_gain: float32 [2048], P('kv'), may hold values from 0.1 to 1.9
- output_weight: bfloat16 [2048, 4096], P('kv', 'tp'), may hold values from -0.125 to 0.125
- mixer_norm_gain: float32 [4096], P('tp'), may hold values from 0.1 to 1.9
- gate_weight: bfloat16 [4096, 11264], P('tp', 'kv'), may hold values from -0.09375 to 0.09375
- up_weight: bfloat16 [4096, 11264], P('tp', 'kv'), may hold values from -0.09375 to 0.09375
- down_weight: bfloat16 [11264, 4096], P('kv', 'tp'), may hold values from -0.0546875 to 0.0546875
Outputs:
- layer_output: float32 [128, 4096], P(None, 'tp')
Inputs may be any that keep to these rules, and one draw needn't show every extreme that they name: `block_lengths`: some sequence has exactly 128 live positions.
All inputs are finite; a program needn't handle non-finite values. No bound on the sum of `block_lengths` on one device may be relied on, other than what follows from the above.
Results may differ from a plain program's by a relative error of at most 0.0078.
Values may be sent and summed in bfloat16 or wider, within the bound.
No kernel may reach another device: no remote copies, remote signals or barrier semaphores. Data moves between devices by JAX's collectives and lax.ppermute only.
A program may use at most 64 MiB of HBM per device.

v0:
```python
import jax
import jax.numpy as jnp
from jax import lax
from jax.sharding import PartitionSpec as P

D = 4096
epsilon = 1e-06


def memory_cell(
    queries,
    new_keys,
    new_values,
    log_input,
    log_forget,
    memory,
    normalizer,
    stabilizer,
    cached_keys,
    cached_values,
    input_pre,
    forget_pre,
    lengths,
    input_bias,
    forget_bias,
):
    positions = jnp.arange(cached_keys.shape[2])
    is_live = (positions[None, :] < lengths[:, None])[:, None, :]
    cached_input = input_pre + input_bias[None, :, None]
    cached_forget = jnp.where(
        is_live, jax.nn.log_sigmoid(forget_pre + forget_bias[None, :, None]), 0.0
    )
    after_mask = (positions[:, None] > positions[None, :]).astype(jnp.float32)
    later_forget = (
        jnp.einsum("bhu,us->bhs", cached_forget, after_mask, precision=lax.Precision.HIGHEST)
        + log_forget[..., None]
    )
    total_forget = jnp.sum(cached_forget, axis=-1) + log_forget
    exponent = jnp.where(is_live, later_forget + cached_input, -jnp.inf)
    carried = total_forget + stabilizer
    stab_max = jnp.maximum(jnp.maximum(jnp.max(exponent, axis=-1), carried), log_input)
    scores = jnp.einsum("bhd,bhsd->bhs", queries, cached_keys, preferred_element_type=jnp.float32)
    block_weight = jnp.exp(exponent - stab_max[..., None]) * scores
    block_probs = block_weight.astype(jnp.bfloat16)
    block_sum = jnp.einsum(
        "bhs,bhsd->bhd", block_probs, cached_values, preferred_element_type=jnp.float32
    )
    query_wide = queries.astype(jnp.float32)
    new_weight = jnp.exp(log_input - stab_max) * jnp.sum(
        query_wide * new_keys.astype(jnp.float32), axis=-1
    )
    state_weight = jnp.exp(carried - stab_max)
    state_sum = jnp.einsum("bhkv,bhk->bhv", memory, query_wide, precision=lax.Precision.HIGHEST)
    state_norm = jnp.sum(normalizer * query_wide, axis=-1)
    numerator = (
        block_sum
        + new_weight[..., None] * new_values.astype(jnp.float32)
        + state_weight[..., None] * state_sum
    )
    denominator = jnp.sum(block_weight, axis=-1) + new_weight + state_weight * state_norm
    return numerator / jnp.maximum(jnp.abs(denominator), 1.0)[..., None]


def head_scale(cell_out, gain):
    return (cell_out * gain.reshape(cell_out.shape[1], cell_out.shape[2])).astype(jnp.bfloat16)


def activate(gate_sum, up_sum, square_sum):
    row_scale = lax.rsqrt(square_sum / D + epsilon)[:, None]
    return (jax.nn.silu(gate_sum * row_scale) * (up_sum * row_scale)).astype(jnp.bfloat16)


def body(
    tokens,
    norm_gain,
    query_weight,
    key_weight,
    value_weight,
    input_gate_weight,
    forget_gate_weight,
    input_gate_bias,
    forget_gate_bias,
    memory_state,
    normalizer_state,
    stabilizer_state,
    block_keys,
    block_values,
    block_input_pre,
    block_forget_pre,
    block_lengths,
    head_norm_gain,
    output_weight,
    mixer_norm_gain,
    gate_weight,
    up_weight,
    down_weight,
):
    seq_rows = block_keys.shape[0]
    heads_dev = block_keys.shape[1]
    head_size = block_keys.shape[3]
    tok_wide = tokens.astype(jnp.float32)
    scaled_in = (tok_wide * norm_gain).astype(jnp.bfloat16)
    square_part = jnp.sum(tok_wide * tok_wide, axis=1)

    def partial_of(weight):
        return jnp.dot(scaled_in, weight, preferred_element_type=jnp.float32)

    query_sum, key_sum, value_sum, input_sum, forget_sum, square_sum = (
        lax.psum_scatter(partial_of(query_weight), "tp", scatter_dimension=0, tiled=True),
        lax.psum_scatter(partial_of(key_weight), "tp", scatter_dimension=0, tiled=True),
        lax.psum_scatter(partial_of(value_weight), "tp", scatter_dimension=0, tiled=True),
        lax.psum_scatter(partial_of(input_gate_weight), "tp", scatter_dimension=0, tiled=True),
        lax.psum_scatter(partial_of(forget_gate_weight), "tp", scatter_dimension=0, tiled=True),
        lax.psum_scatter(square_part, "tp", scatter_dimension=0, tiled=True),
    )
    first_scale = lax.rsqrt(square_sum / D + epsilon)[:, None]
    queries = (
        (query_sum * first_scale * head_size ** (-0.5))
        .astype(jnp.bfloat16)
        .reshape(seq_rows, heads_dev, head_size)
    )
    new_keys = (key_sum * first_scale).astype(jnp.bfloat16).reshape(seq_rows, heads_dev, head_size)
    new_values = (
        (value_sum * first_scale).astype(jnp.bfloat16).reshape(seq_rows, heads_dev, head_size)
    )
    head_start = lax.axis_index("kv") * heads_dev
    log_input = (
        lax.dynamic_slice_in_dim(input_sum * first_scale, head_start, heads_dev, 1)
        + input_gate_bias
    )
    log_forget = jax.nn.log_sigmoid(
        lax.dynamic_slice_in_dim(forget_sum * first_scale, head_start, heads_dev, 1)
        + forget_gate_bias
    )
    cell_out = memory_cell(
        queries,
        new_keys,
        new_values,
        log_input,
        log_forget,
        memory_state,
        normalizer_state,
        stabilizer_state,
        block_keys,
        block_values,
        block_input_pre,
        block_forget_pre,
        block_lengths,
        input_gate_bias,
        forget_gate_bias,
    )
    head_out = head_scale(cell_out, head_norm_gain).reshape(seq_rows, heads_dev * head_size)
    attended_part = jnp.dot(
        lax.all_gather(head_out, "tp", axis=0, tiled=True),
        output_weight,
        preferred_element_type=jnp.float32,
    )
    attended = lax.psum(attended_part, "kv")
    res_wide = tok_wide + attended
    mid_square = jnp.sum(res_wide * res_wide, axis=1)
    mid_scaled = (res_wide * mixer_norm_gain).astype(jnp.bfloat16)
    gate_part = jnp.dot(mid_scaled, gate_weight, preferred_element_type=jnp.float32)
    up_part = jnp.dot(mid_scaled, up_weight, preferred_element_type=jnp.float32)
    gate_sum, up_sum, mid_sum = lax.psum((gate_part, up_part, mid_square), "tp")
    hidden = activate(gate_sum, up_sum, mid_sum)
    down_part = jnp.dot(hidden, down_weight, preferred_element_type=jnp.float32)
    mixed = lax.psum(down_part, "kv")
    return res_wide + mixed


def solution(mesh):
    placed = (
        P(None, "tp"),
        P("tp"),
        P("tp", "kv"),
        P("tp", "kv"),
        P("tp", "kv"),
        P("tp", None),
        P("tp", None),
        P("kv"),
        P("kv"),
        P("tp", "kv", None, None),
        P("tp", "kv", None),
        P("tp", "kv"),
        P("tp", "kv", None, None),
        P("tp", "kv", None, None),
        P("tp", "kv", None),
        P("tp", "kv", None),
        P("tp"),
        P("kv"),
        P("kv", "tp"),
        P("tp"),
        P("tp", "kv"),
        P("tp", "kv"),
        P("kv", "tp"),
    )
    return jax.shard_map(body, mesh=mesh, in_specs=placed, out_specs=P(None, "tp"), check_vma=False)
```

profile of v0, /device:TPU:0, one launch (start us, length us, event | category | flops | bytes accessed | tf_op | source)
XLA Modules:
  0.0 376.3 jit_solution(17206025061885807073)
XLA Ops:
  6.6 1.9 fusion.16
  8.5 1.7 fusion.14
  10.3 2.1 fusion.12
  12.5 2.1 fusion.10
  14.6 0.9 fusion.8
  15.8 18.1 %all-reduce = f32[128]{0:T(128)S(1)} all-reduce(f32[128]{0:T(128)S(1)} %fusion.4), channel_id=3, replica_groups=mesh['kv'=4,'tp'=8] {'tp'}, use_global_device_ids=true, to_apply=%region_2.0.clone | all-reduce | flops 128 | bytes 1024
  34.6 1.3 dynamic-slice
  36.7 0.9 fusion.32
  37.7 5.3 %reduce-scatter.16.cloned.1.call-done = f32[16,16]{1,0:T(8,128)} async-done(((f32[128,16]{1,0:T(8,128)}), f32[16,16]{1,0:T(8,128)}) %reduce-scatter.16.cloned.1.call-update) | async-done | bytes 1040
  43.9 29.9 %reduce-scatter.18.cloned.1.call-done = f32[16,16]{1,0:T(8,128)} async-done(((f32[128,16]{1,0:T(8,128)}), f32[16,16]{1,0:T(8,128)}) %reduce-scatter.18.cloned.1.call-update) | async-done | bytes 1040
  74.6 1.6 fusion.34
  76.9 27.9 %reduce-scatter.10.cloned.1.call-done = f32[16,512]{1,0:T(8,128)} async-done(((f32[128,512]{1,0:T(8,128)}), f32[16,512]{1,0:T(8,128)}) %reduce-scatter.10.cloned.1.call-update) | async-done | bytes 32784 | tf_op jit(solution)/shard_map/reduce_scatter | solution.py:109
  104.9 31.1 %reduce-scatter.12.cloned.1.call-done = f32[16,512]{1,0:T(8,128)} async-done(((f32[128,512]{1,0:T(8,128)}), f32[16,512]{1,0:T(8,128)}) %reduce-scatter.12.cloned.1.call-update) | async-done | bytes 32784 | tf_op jit(solution)/shard_map/reduce_scatter | solution.py:110
  136.0 31.1 %reduce-scatter.14.cloned.1.call-done = f32[16,512]{1,0:T(8,128)} async-done(((f32[128,512]{1,0:T(8,128)}), f32[16,512]{1,0:T(8,128)}) %reduce-scatter.14.cloned.1.call-update) | async-done | bytes 32784 | tf_op jit(solution)/shard_map/reduce_scatter | solution.py:111
  167.0 1.5 fusion.25
  170.8 4.9 %fusion.36 = f32[16,4,1,128]{3,2,1,0:T(1,128)} fusion(bf16[16,4,128,1]{2,3,1,0:T(2,128)(2,1)S(1)} %reshape.54, f32[16,4,128,128]{3,2,1,0:T(8,128)} %param.32), kind=kOutput, calls=%fused_computation.61 | convolution fusion | flops 12582912 | bytes 4243456 | tf_op jit(solution)/shard_map/bhkv,bhk->bhv/dot_general | solution.py:53
  175.8 2.0 fusion.35
  178.8 1.3 copy.52
  180.1 1.3 copy.49
  181.5 1.3 copy.50
  182.8 1.4 reshape.46
  184.2 2.3 fusion.22
  186.7 14.0 %all_gather.3 = bf16[128,512]{1,0:T(8,128)(2,1)S(1)} all-gather(bf16[16,512]{1,0:T(8,128)(2,1)S(1)} %bitcast.45), channel_id=1, replica_groups=mesh['kv'=4,'tp'=8] {'tp'}, dimensions={0}, use_global_device_ids=true | all-gather | bytes 147456 | tf_op jit(solution)/shard_map/all_gather | solution.py:154
  201.7 41.3 %all-reduce.6.cloned.1.call-done = f32[128,512]{1,0:T(8,128)} async-done(((f32[128,512]{1,0:T(8,128)}), f32[128,512]{1,0:T(8,128)}) %all-reduce.6.cloned.1.call-update) | async-done | bytes 262160 | tf_op jit(solution)/shard_map/psum | solution.py:158
  243.0 1.1 multiply_reduce_fusion
  244.1 1.7 fusion.39
  246.4 1.7 fusion.38
  248.2 16.2 %psum.37 = f32[128]{0:T(128)S(1)} all-reduce(f32[128]{0:T(128)S(1)} %get-tuple-element.12), channel_id=1, replica_groups=mesh['kv'=4,'tp'=8] {'tp'}, use_global_device_ids=true, to_apply=%region_15.16 | all-reduce | flops 128 | bytes 1024 | tf_op jit(solution)/shard_map/psum | solution.py:164
  264.4 56.5 %all-reduce.10.cloned.1.call-done = (f32[128,2816]{1,0:T(8,128)}, f32[128,2816]{1,0:T(8,128)}) async-done(((f32[128,2816]{1,0:T(8,128)}, f32[128,2816]{1,0:T(8,128)}), (f32[128,2816]{1,0:T(8,128)}, f32[128,2816]{1,0:T(8,128)})) %all-reduce.10.cloned.1.call-update) | async-done | bytes 2883600 | tf_op jit(solution)/shard_map/psum | solution.py:164
  320.9 4.2 %fusion.2 = f32[128,512]{1,0:T(8,128)} fusion(bf16[2816,512]{1,0:T(8,128)(2,1)} %param.45, f32[128,2816]{1,0:T(8,128)} %get-tuple-element.7, f32[128,2816]{1,0:T(8,128)} %get-tuple-element.8, f32[128]{0:T(128)S(1)} %add_rsqrt_fusion), kind=kOutput, calls=%fused_computation.4 | convolution fusion | flops 371982336 | bytes 6029824 | tf_op jit(solution)/shard_map/dot_general | solution.py:166
  325.1 42.7 %all-reduce.8.cloned.1.call-done = f32[128,512]{1,0:T(8,128)} async-done(((f32[128,512]{1,0:T(8,128)}), f32[128,512]{1,0:T(8,128)}) %all-reduce.8.cloned.1.call-update) | async-done | bytes 262160 | tf_op jit(solution)/shard_map/psum | solution.py:167
  367.8 1.7 fusion.5
  (103 shorter events, 8.8 us)
Async XLA Ops:
  6.5 237.5 %copy-start = (bf16[512,2816]{1,0:T(8,128)(2,1)S(1)}, bf16[512,2816]{1,0:T(8,128)(2,1)}, u32[]{:S(2)}) copy-start(bf16[512,2816]{1,0:T(8,128)(2,1)} %param.44) | copy-start | bytes 8650756
  6.5 8.1 %copy-start.1 = (bf16[128,512]{1,0:T(8,128)(2,1)S(1)}, bf16[128,512]{1,0:T(8,128)(2,1)}, u32[]{:S(2)}) copy-start(bf16[128,512]{1,0:T(8,128)(2,1)} %param.23) | copy-start | bytes 393220
  6.5 8.1 %copy-start.10 = (f32[512]{0:T(512)S(1)}, f32[512]{0:T(512)}, u32[]{:S(2)}) copy-start(f32[512]{0:T(512)} %param.24) | copy-start | bytes 6148
  6.5 8.1 %copy-start.5 = (bf16[512,512]{1,0:T(8,128)(2,1)S(1)}, bf16[512,512]{1,0:T(8,128)(2,1)}, u32[]{:S(2)}) copy-start(bf16[512,512]{1,0:T(8,128)(2,1)} %param.27) | copy-start | bytes 1572868
  6.5 36.4 %reduce-scatter.16.cloned.1.call-start = ((), (), s32[]{:S(2)}) async-start(), calls=%async_computation.10 | async-start | bytes 73728
  8.5 28.2 %copy-start.22 = (f32[4]{0:T(128)S(1)}, f32[4]{0:T(128)}, u32[]{:S(2)}) copy-start(f32[4]{0:T(128)} %param.31) | copy-start | bytes 52
  8.5 66.2 %copy-start.31 = (f32[4]{0:T(128)S(1)}, f32[4]{0:T(128)}, u32[]{:S(2)}) copy-start(f32[4]{0:T(128)} %param.30) | copy-start | bytes 52
  8.5 65.3 %reduce-scatter.18.cloned.1.call-start = ((), (), s32[]{:S(2)}) async-start(), calls=%async_computation.11 | async-start | bytes 73728
  10.2 66.0 %copy-start.26 = (f32[16,4]{0,1:T(4,128)S(1)}, f32[16,4]{0,1:T(4,128)}, u32[]{:S(2)}) copy-start(f32[16,4]{0,1:T(4,128)} %param.34) | copy-start | bytes 772
  10.3 94.6 %reduce-scatter.10.cloned.1.call-start = ((), (), s32[]{:S(2)}) async-start(), calls=%async_computation.5 | async-start | bytes 294912 | tf_op jit(solution)/shard_map/reduce_scatter | solution.py:109
  12.4 123.5 %reduce-scatter.12.cloned.1.call-start = ((), (), s32[]{:S(2)}) async-start(), calls=%async_computation.6 | async-start | bytes 294912 | tf_op jit(solution)/shard_map/reduce_scatter | solution.py:110
  14.6 152.5 %reduce-scatter.14.cloned.1.call-start = ((), (), s32[]{:S(2)}) async-start(), calls=%async_computation.7 | async-start | bytes 294912 | tf_op jit(solution)/shard_map/reduce_scatter | solution.py:111
  15.6 227.4 %all-reduce.6.cloned.1.call-start = ((), (), s32[]{:S(2)}) async-start(), calls=%async_computation.8 | async-start | bytes 524288 | tf_op jit(solution)/shard_map/psum | solution.py:158
  36.7 131.8 %copy-start.24 = (f32[16]{0:T(128)}, f32[16]{0:T(128)S(1)}, u32[]{:S(2)}) copy-start(f32[16]{0:T(128)S(1)} %fusion.30) | copy-start | bytes 196
  37.6 130.9 %copy-start.17 = (f32[16,4]{0,1:T(4,128)}, f32[16,4]{0,1:T(4,128)S(1)}, u32[]{:S(2)}) copy-start(f32[16,4]{0,1:T(4,128)S(1)} %fusion.32) | copy-start | bytes 772
  43.8 124.7 %copy-start.14 = (f32[16,4]{0,1:T(4,128)}, f32[16,4]{0,1:T(4,128)S(1)}, u32[]{:S(2)}) copy-start(f32[16,4]{0,1:T(4,128)S(1)} %copy.64) | copy-start | bytes 772
  74.6 93.9 %copy-start.19 = (f32[16,4]{0,1:T(4,128)}, f32[16,4]{0,1:T(4,128)S(1)}, u32[]{:S(2)}) copy-start(f32[16,4]{0,1:T(4,128)S(1)} %copy.65) | copy-start | bytes 772
  170.8 4.9 %copy-start.3 = (bf16[16,4,128,128]{3,2,1,0:T(8,128)(2,1)S(1)}, bf16[16,4,128,128]{3,2,1,0:T(8,128)(2,1)}, u32[]{:S(2)}) copy-start(bf16[16,4,128,128]{3,2,1,0:T(8,128)(2,1)} %param.35) | copy-start | bytes 6291460
  175.7 2.3 copy-start.15
  175.7 2.3 copy-start.18
  175.7 2.3 copy-start.20
  175.8 24.9 %copy-start.6 = (bf16[512,512]{1,0:T(8,128)(2,1)S(1)}, bf16[512,512]{1,0:T(8,128)(2,1)}, u32[]{:S(2)}) copy-start(bf16[512,512]{1,0:T(8,128)(2,1)} %param.41) | copy-start | bytes 1572868
  184.2 2.3 copy-start.8
  184.2 2.3 copy-start.9
  184.2 2.3 copy-start.11
  184.2 2.3 copy-start.12
  184.2 2.3 copy-start.13
  184.2 2.3 copy-start.30
  201.6 119.3 %all-reduce.10.cloned.1.call-start = ((), (), s32[]{:S(2)}) async-start(), calls=%async_computation.12 | async-start | bytes 5767168 | tf_op jit(solution)/shard_map/psum | solution.py:164
  244.0 2.3 copy-start.2
  248.1 119.7 %all-reduce.8.cloned.1.call-start = ((), (), s32[]{:S(2)}) async-start(), calls=%async_computation.9 | async-start | bytes 524288 | tf_op jit(solution)/shard_map/psum | solution.py:167
  320.9 46.9 %copy-start.4 = (f32[128,512]{1,0:T(8,128)S(1)}, f32[128,512]{1,0:T(8,128)}, u32[]{:S(2)}) copy-start(f32[128,512]{1,0:T(8,128)} %all-reduce.6.cloned.1.call-done) | copy-start | bytes 786436
  (9 other events, 20.1 us)
Sparse Core Ops, SparseCore 0:
  9.6 33.3 reduce-scatter.15
  45.2 28.5 reduce-scatter.17
  76.0 28.8 reduce-scatter.9
  107.0 28.9 reduce-scatter.11
  138.0 28.9 reduce-scatter.13
  201.8 41.1 all-reduce.5
  248.2 72.6 all-reduce.9
  325.2 42.5 all-reduce.7
where the time goes:
time: 377 us; the launch traced here: 376 us
  waiting for transfers between devices  266 us (71%)
  blocking collectives  48.3 us (13%)
  matrix products  28 us (7%)
  between operations  14.5 us (4%)
  local copies, waits for them, and re-layouts  10.6 us (3%)
  other arithmetic  8.77 us (2%)
    psum x1, waiting for transfers between devices, body(): gate_sum, up_sum, mid_sum = lax.psum((gate_part, up_part, mid_square), 'tp')  56.5 us
    psum x1, waiting for transfers between devices, body(): mixed = lax.psum(down_part, 'kv')  42.7 us
    psum x1, waiting for transfers between devices, body(): attended = lax.psum(attended_part, 'kv')  41.3 us
    unnamed x10, waiting for transfers between devices  35.3 us
    reduce_scatter x1, waiting for transfers between devices, body(): lax.psum_scatter(partial_of(key_weight), 'tp', scatter_dimension=0, tiled...  31.1 us
    reduce_scatter x1, waiting for transfers between devices, body(): lax.psum_scatter(partial_of(value_weight), 'tp', scatter_dimension=0, til...  31.1 us
    reduce_scatter x1, waiting for transfers between devices, body(): lax.psum_scatter(partial_of(query_weight), 'tp', scatter_dimension=0, til...  27.9 us
    unnamed x1, blocking collectives  18.1 us
  transfers between devices with their start and end apart: 8, of which 8 were waited for; matrix products, arithmetic and copies ran while one was open for 4% of the time, Pallas kernels for 0%

commit v1 on v0

--- a/solution.py
+++ b/solution.py
@@ -155,7 +155,7 @@
         output_weight,
         preferred_element_type=jnp.float32,
     )
-    attended = lax.psum(attended_part, "kv")
+    attended = jnp.sum(lax.all_gather(attended_part, "kv"), axis=0)
     res_wide = tok_wide + attended
     mid_square = jnp.sum(res_wide * res_wide, axis=1)
     mid_scaled = (res_wide * mixer_norm_gain).astype(jnp.bfloat16)

time: 377 us -> 361 us (0.958)
  waiting for transfers between devices: 266 us -> 249 us
    psum x1 -> x0, waiting for transfers between devices: 41.3 us -> none  [body(): attended = lax.psum(attended_part, 'kv')]
    all_gather x0 -> x1, waiting for transfers between devices: none -> 24.7 us  [body(): attended = jnp.sum(lax.all_gather(attended_part, 'kv'), axis=0)]
where the time goes in v1:
time: 361 us; the launch traced here: 360 us
  waiting for transfers between devices  249 us (69%)
  blocking collectives  48.7 us (13%)
  matrix products  27.9 us (8%)
  between operations  14.6 us (4%)
  local copies, waits for them, and re-layouts  10.6 us (3%)
  other arithmetic  9.14 us (3%)
    psum x1, waiting for transfers between devices, body(): gate_sum, up_sum, mid_sum = lax.psum((gate_part, up_part, mid_square), 'tp')  56.1 us
    psum x1, waiting for transfers between devices, body(): mixed = lax.psum(down_part, 'kv')  42.7 us
    unnamed x10, waiting for transfers between devices  35.3 us
    reduce_scatter x1, waiting for transfers between devices, body(): lax.psum_scatter(partial_of(key_weight), 'tp', scatter_dimension=0, tiled...  31.1 us
    reduce_scatter x1, waiting for transfers between devices, body(): lax.psum_scatter(partial_of(value_weight), 'tp', scatter_dimension=0, til...  31.1 us
    reduce_scatter x1, waiting for transfers between devices, body(): lax.psum_scatter(partial_of(query_weight), 'tp', scatter_dimension=0, til...  27.9 us
    all_gather x1, waiting for transfers between devices, body(): attended = jnp.sum(lax.all_gather(attended_part, 'kv'), axis=0)  24.7 us
    unnamed x1, blocking collectives  18.1 us
  transfers between devices with their start and end apart: 8, of which 8 were waited for; matrix products, arithmetic and copies ran while one was open for 4% of the time, Pallas kernels for 0%

profile of v1, /device:TPU:0, one launch (start us, length us, event | category | flops | bytes accessed | tf_op | source)
XLA Modules:
  0.0 360.2 jit_solution(15451674183434411174)
XLA Ops:
  6.6 1.9 fusion.16
  8.5 1.7 fusion.14
  10.3 2.1 fusion.12
  12.5 2.1 fusion.10
  14.6 0.9 fusion.8
  15.8 18.1 %all-reduce = f32[128]{0:T(128)S(1)} all-reduce(f32[128]{0:T(128)S(1)} %fusion.4), channel_id=4, replica_groups=mesh['kv'=4,'tp'=8] {'tp'}, use_global_device_ids=true, to_apply=%region_2.0.clone | all-reduce | flops 128 | bytes 1024
  34.6 1.3 dynamic-slice
  36.7 0.9 fusion.32
  37.7 5.3 %reduce-scatter.16.cloned.1.call-done = f32[16,16]{1,0:T(8,128)} async-done(((f32[128,16]{1,0:T(8,128)}), f32[16,16]{1,0:T(8,128)}) %reduce-scatter.16.cloned.1.call-update) | async-done | bytes 1040
  43.9 29.9 %reduce-scatter.18.cloned.1.call-done = f32[16,16]{1,0:T(8,128)} async-done(((f32[128,16]{1,0:T(8,128)}), f32[16,16]{1,0:T(8,128)}) %reduce-scatter.18.cloned.1.call-update) | async-done | bytes 1040
  74.6 1.6 fusion.34
  76.9 27.9 %reduce-scatter.10.cloned.1.call-done = f32[16,512]{1,0:T(8,128)} async-done(((f32[128,512]{1,0:T(8,128)}), f32[16,512]{1,0:T(8,128)}) %reduce-scatter.10.cloned.1.call-update) | async-done | bytes 32784 | tf_op jit(solution)/shard_map/reduce_scatter | solution.py:109
  104.9 31.1 %reduce-scatter.12.cloned.1.call-done = f32[16,512]{1,0:T(8,128)} async-done(((f32[128,512]{1,0:T(8,128)}), f32[16,512]{1,0:T(8,128)}) %reduce-scatter.12.cloned.1.call-update) | async-done | bytes 32784 | tf_op jit(solution)/shard_map/reduce_scatter | solution.py:110
  136.0 31.1 %reduce-scatter.14.cloned.1.call-done = f32[16,512]{1,0:T(8,128)} async-done(((f32[128,512]{1,0:T(8,128)}), f32[16,512]{1,0:T(8,128)}) %reduce-scatter.14.cloned.1.call-update) | async-done | bytes 32784 | tf_op jit(solution)/shard_map/reduce_scatter | solution.py:111
  167.0 1.5 fusion.25
  170.8 4.9 %fusion.36 = f32[16,4,1,128]{3,2,1,0:T(1,128)} fusion(bf16[16,4,128,1]{2,3,1,0:T(2,128)(2,1)S(1)} %reshape.55, f32[16,4,128,128]{3,2,1,0:T(8,128)} %param.32), kind=kOutput, calls=%fused_computation.61 | convolution fusion | flops 12582912 | bytes 4243456 | tf_op jit(solution)/shard_map/bhkv,bhk->bhv/dot_general | solution.py:53
  175.8 2.0 fusion.35
  178.8 1.3 copy.52
  180.1 1.3 copy.49
  181.5 1.3 copy.50
  182.8 1.4 reshape.46
  184.2 2.3 fusion.22
  186.7 14.0 %all_gather.9 = bf16[128,512]{1,0:T(8,128)(2,1)S(1)} all-gather(bf16[16,512]{1,0:T(8,128)(2,1)S(1)} %bitcast.47), channel_id=1, replica_groups=mesh['kv'=4,'tp'=8] {'tp'}, dimensions={0}, use_global_device_ids=true | all-gather | bytes 147456 | tf_op jit(solution)/shard_map/all_gather | solution.py:154
  201.7 24.7 %all-gather.3.cloned.1.call-done = f32[512,512]{1,0:T(8,128)} async-done(((f32[128,512]{1,0:T(8,128)}), f32[512,512]{1,0:T(8,128)}) %all-gather.3.cloned.1.call-update) | async-done | bytes 1048592 | tf_op jit(solution)/shard_map/all_gather | solution.py:158
  226.4 1.3 reduce_sum.68
  227.9 1.7 fusion.39
  230.2 1.7 fusion.38
  232.0 16.6 %psum.29 = f32[128]{0:T(128)S(1)} all-reduce(f32[128]{0:T(128)S(1)} %get-tuple-element.12), channel_id=1, replica_groups=mesh['kv'=4,'tp'=8] {'tp'}, use_global_device_ids=true, to_apply=%region_15.16 | all-reduce | flops 128 | bytes 1024 | tf_op jit(solution)/shard_map/psum | solution.py:164
  248.7 56.1 %all-reduce.7.cloned.1.call-done = (f32[128,2816]{1,0:T(8,128)}, f32[128,2816]{1,0:T(8,128)}) async-done(((f32[128,2816]{1,0:T(8,128)}, f32[128,2816]{1,0:T(8,128)}), (f32[128,2816]{1,0:T(8,128)}, f32[128,2816]{1,0:T(8,128)})) %all-reduce.7.cloned.1.call-update) | async-done | bytes 2883600 | tf_op jit(solution)/shard_map/psum | solution.py:164
  304.8 4.1 %fusion.2 = f32[128,512]{1,0:T(8,128)} fusion(bf16[2816,512]{1,0:T(8,128)(2,1)} %param.45, f32[128,2816]{1,0:T(8,128)} %get-tuple-element.7, f32[128,2816]{1,0:T(8,128)} %get-tuple-element.8, f32[128]{0:T(128)S(1)} %add_rsqrt_fusion), kind=kOutput, calls=%fused_computation.4 | convolution fusion | flops 371982336 | bytes 6029824 | tf_op jit(solution)/shard_map/dot_general | solution.py:166
  308.9 42.7 %all-reduce.5.cloned.1.call-done = f32[128,512]{1,0:T(8,128)} async-done(((f32[128,512]{1,0:T(8,128)}), f32[128,512]{1,0:T(8,128)}) %all-reduce.5.cloned.1.call-update) | async-done | bytes 262160 | tf_op jit(solution)/shard_map/psum | solution.py:167
  351.6 1.7 fusion.5
  (104 shorter events, 8.9 us)
Async XLA Ops:
  6.5 221.4 %copy-start = (bf16[512,2816]{1,0:T(8,128)(2,1)S(1)}, bf16[512,2816]{1,0:T(8,128)(2,1)}, u32[]{:S(2)}) copy-start(bf16[512,2816]{1,0:T(8,128)(2,1)} %param.44) | copy-start | bytes 8650756
  6.5 8.1 %copy-start.1 = (bf16[128,512]{1,0:T(8,128)(2,1)S(1)}, bf16[128,512]{1,0:T(8,128)(2,1)}, u32[]{:S(2)}) copy-start(bf16[128,512]{1,0:T(8,128)(2,1)} %param.23) | copy-start | bytes 393220
  6.5 8.1 %copy-start.9 = (f32[512]{0:T(512)S(1)}, f32[512]{0:T(512)}, u32[]{:S(2)}) copy-start(f32[512]{0:T(512)} %param.24) | copy-start | bytes 6148
  6.5 8.1 %copy-start.4 = (bf16[512,512]{1,0:T(8,128)(2,1)S(1)}, bf16[512,512]{1,0:T(8,128)(2,1)}, u32[]{:S(2)}) copy-start(bf16[512,512]{1,0:T(8,128)(2,1)} %param.27) | copy-start | bytes 1572868
  6.5 36.4 %reduce-scatter.16.cloned.1.call-start = ((), (), s32[]{:S(2)}) async-start(), calls=%async_computation.10 | async-start | bytes 73728
  8.5 28.2 %copy-start.21 = (f32[4]{0:T(128)S(1)}, f32[4]{0:T(128)}, u32[]{:S(2)}) copy-start(f32[4]{0:T(128)} %param.31) | copy-start | bytes 52
  8.5 66.2 %copy-start.31 = (f32[4]{0:T(128)S(1)}, f32[4]{0:T(128)}, u32[]{:S(2)}) copy-start(f32[4]{0:T(128)} %param.30) | copy-start | bytes 52
  8.5 65.3 %reduce-scatter.18.cloned.1.call-start = ((), (), s32[]{:S(2)}) async-start(), calls=%async_computation.11 | async-start | bytes 73728
  10.2 66.0 %copy-start.25 = (f32[16,4]{0,1:T(4,128)S(1)}, f32[16,4]{0,1:T(4,128)}, u32[]{:S(2)}) copy-start(f32[16,4]{0,1:T(4,128)} %param.34) | copy-start | bytes 772
  10.3 94.6 %reduce-scatter.10.cloned.1.call-start = ((), (), s32[]{:S(2)}) async-start(), calls=%async_computation.5 | async-start | bytes 294912 | tf_op jit(solution)/shard_map/reduce_scatter | solution.py:109
  12.4 123.5 %reduce-scatter.12.cloned.1.call-start = ((), (), s32[]{:S(2)}) async-start(), calls=%async_computation.6 | async-start | bytes 294912 | tf_op jit(solution)/shard_map/reduce_scatter | solution.py:110
  14.6 152.5 %reduce-scatter.14.cloned.1.call-start = ((), (), s32[]{:S(2)}) async-start(), calls=%async_computation.7 | async-start | bytes 294912 | tf_op jit(solution)/shard_map/reduce_scatter | solution.py:111
  15.6 210.8 %all-gather.3.cloned.1.call-start = ((), (), s32[]{:S(2)}) async-start(), calls=%async_computation.9 | async-start | bytes 1310720 | tf_op jit(solution)/shard_map/all_gather | solution.py:158
  36.7 131.8 %copy-start.23 = (f32[16]{0:T(128)}, f32[16]{0:T(128)S(1)}, u32[]{:S(2)}) copy-start(f32[16]{0:T(128)S(1)} %fusion.30) | copy-start | bytes 196
  37.6 130.9 %copy-start.16 = (f32[16,4]{0,1:T(4,128)}, f32[16,4]{0,1:T(4,128)S(1)}, u32[]{:S(2)}) copy-start(f32[16,4]{0,1:T(4,128)S(1)} %fusion.32) | copy-start | bytes 772
  43.8 124.7 %copy-start.13 = (f32[16,4]{0,1:T(4,128)}, f32[16,4]{0,1:T(4,128)S(1)}, u32[]{:S(2)}) copy-start(f32[16,4]{0,1:T(4,128)S(1)} %copy.64) | copy-start | bytes 772
  74.6 93.9 %copy-start.18 = (f32[16,4]{0,1:T(4,128)}, f32[16,4]{0,1:T(4,128)S(1)}, u32[]{:S(2)}) copy-start(f32[16,4]{0,1:T(4,128)S(1)} %copy.65) | copy-start | bytes 772
  170.8 4.9 %copy-start.3 = (bf16[16,4,128,128]{3,2,1,0:T(8,128)(2,1)S(1)}, bf16[16,4,128,128]{3,2,1,0:T(8,128)(2,1)}, u32[]{:S(2)}) copy-start(bf16[16,4,128,128]{3,2,1,0:T(8,128)(2,1)} %param.35) | copy-start | bytes 6291460
  175.7 2.3 copy-start.14
  175.7 2.3 copy-start.17
  175.7 2.3 copy-start.19
  175.8 24.9 %copy-start.5 = (bf16[512,512]{1,0:T(8,128)(2,1)S(1)}, bf16[512,512]{1,0:T(8,128)(2,1)}, u32[]{:S(2)}) copy-start(bf16[512,512]{1,0:T(8,128)(2,1)} %param.41) | copy-start | bytes 1572868
  184.2 2.3 copy-start.7
  184.2 2.3 copy-start.8
  184.2 2.3 copy-start.10
  184.2 2.3 copy-start.11
  184.2 2.4 copy-start.12
  184.2 2.4 copy-start.29
  186.5 41.3 %copy-start.30 = (f32[512]{0:T(512)S(1)}, f32[512]{0:T(512)}, u32[]{:S(2)}) copy-start(f32[512]{0:T(512)} %param.42) | copy-start | bytes 6148
  201.6 103.1 %all-reduce.7.cloned.1.call-start = ((), (), s32[]{:S(2)}) async-start(), calls=%async_computation.12 | async-start | bytes 5767168 | tf_op jit(solution)/shard_map/psum | solution.py:164
  227.9 2.3 copy-start.2
  232.0 119.7 %all-reduce.5.cloned.1.call-start = ((), (), s32[]{:S(2)}) async-start(), calls=%async_computation.8 | async-start | bytes 524288 | tf_op jit(solution)/shard_map/psum | solution.py:167
  (9 other events, 20.1 us)
Sparse Core Ops, SparseCore 0:
  9.6 33.3 reduce-scatter.15
  45.2 28.5 reduce-scatter.17
  76.0 28.8 reduce-scatter.9
  107.0 28.9 reduce-scatter.11
  138.0 28.9 reduce-scatter.13
  201.8 24.6 all-gather.2
  232.1 72.6 all-reduce.6
  309.0 42.5 all-reduce.4
